TPU v7x, 32 devices: a whole 2x2x4 slice. The times are simulated.
32 devices in a mesh: sp: 8 (over z, core), tp: 4 (over y, x).
Axes of the slice: x: 2, y: 2, z: 4, core: 2. Of those that a mesh axis runs over, the one named last changes fastest.
Arguments:
- resid: bfloat16 [1536, 2048], P('sp', 'tp'), may hold values from -12 to 12
- conv_value: bfloat16 [1536, 2048], P('sp', 'tp'), may hold values from -80 to 80
- conv_gate: bfloat16 [1536, 2048], P('sp', 'tp'), may hold values from -6 to 6
- depth_kernel: float32 [31, 2048], P(None, 'tp'), may hold values from -1 to 1
- chan_gain: float32 [2048], P('tp'), may hold values from 0.1 to 1.9
- point_weight: bfloat16 [2048, 2048], P('tp'), may hold values from -0.125 to 0.125
- mix_gain: float32 [2048], replicated, may hold values from 0.1 to 1.9
- out_weight: bfloat16 [2048, 2048], P(None, 'tp'), may hold values from -0.125 to 0.125
- norm_gain: float32 [2048], P('tp'), may hold values from 0.1 to 1.9
- route_ids: int32 [1536, 4], P('sp'), may hold values from 0 to 31, all different within a row; in each aligned block of 192 rows (0 to 191, 192 to 383, ...) at most 32 rows name the same one
- route_weights: float32 [1536, 4], P('sp'), may hold values from 0.05 to 0.5
- gate_experts: bfloat16 [32, 2048, 4096], P('sp', None, 'tp'), may hold values from -0.3125 to 0.3125
- up_experts: bfloat16 [32, 2048, 4096], P('sp', None, 'tp'), may hold values from -0.3125 to 0.3125
- down_experts: bfloat16 [32, 4096, 2048], P('sp', 'tp'), may hold values from -0.09375 to 0.09375
Outputs:
- result: bfloat16 [1536, 2048], P('sp', 'tp')
Inputs may be any that keep to these rules, and one draw needn't show every extreme that they name: `route_ids`: each row names 4 different experts; among the 192 rows of one index of sp no expert is named by more than 32 rows, and in some such block an expert is named by exactly 32.
All inputs are finite; a program needn't handle non-finite values.
Results may differ from a plain program's by a relative error of at most 0.024.
Values may be sent and summed in bfloat16 or wider, within the bound.
No kernel may reach another device: no remote copies, remote signals or barrier semaphores. Data moves between devices by JAX's collectives and lax.ppermute only.
A program may use at most 128 MiB of HBM per device.

v0:
```python
import jax
import jax.numpy as jnp
from jax import lax
from jax.sharding import PartitionSpec as P

E = 32
TOPK = 4
CAP = 32
epsilon = 1e-05
clamp_limit = 7.0
swish_slope = 1.702


def from_behind(block, axis, distance):
    devices = range(lax.axis_size(axis))
    route = [(i - distance, i) for i in devices if i - distance in devices]
    return lax.ppermute(block, axis, route)


def shards(
    resid,
    conv_value,
    conv_gate,
    depth_kernel,
    chan_gain,
    point_weight,
    mix_gain,
    out_weight,
    norm_gain,
    route_ids,
    route_weights,
    gate_experts,
    up_experts,
    down_experts,
):
    tok_rows, chan_local = conv_value.shape
    feat_local = resid.shape[1]
    lookback = depth_kernel.shape[0] - 1
    gated = (conv_value.astype(jnp.float32) * jax.nn.sigmoid(conv_gate.astype(jnp.float32))).astype(
        jnp.bfloat16
    )
    earlier = from_behind(gated[tok_rows - lookback :], "sp", 1)
    padded = jnp.concatenate([earlier, gated], axis=0)
    conv = jnp.zeros((tok_rows, chan_local), jnp.float32)
    for tap in range(lookback + 1):
        conv = conv + padded[tap : tap + tok_rows].astype(jnp.float32) * depth_kernel[tap]
    chan_total = chan_local * lax.axis_size("tp")
    row_sums, row_squares = lax.psum((jnp.sum(conv, axis=1), jnp.sum(conv * conv, axis=1)), "tp")
    row_mean = row_sums / chan_total
    row_var = row_squares / chan_total - row_mean * row_mean
    act = jax.nn.silu(
        (conv - row_mean[:, None]) * lax.rsqrt(row_var[:, None] + epsilon) * chan_gain
    ).astype(jnp.bfloat16)
    point = lax.psum_scatter(
        jnp.dot(act, point_weight, preferred_element_type=jnp.float32).astype(jnp.bfloat16),
        "tp",
        scatter_dimension=0,
        tiled=True,
    ).astype(jnp.float32)
    mixed = (
        point * lax.rsqrt(jnp.mean(point * point, axis=1, keepdims=True) + epsilon) * mix_gain
    ).astype(jnp.bfloat16)
    branch = jnp.dot(
        lax.all_gather(mixed, "tp", axis=0, tiled=True),
        out_weight,
        preferred_element_type=jnp.float32,
    )
    middle = (resid.astype(jnp.float32) + branch).astype(jnp.bfloat16)
    middle32 = middle.astype(jnp.float32)
    feat_total = feat_local * lax.axis_size("tp")
    squares = lax.psum(jnp.sum(middle32 * middle32, axis=1), "tp")
    normed = (middle32 * lax.rsqrt(squares[:, None] / feat_total + epsilon) * norm_gain).astype(
        jnp.bfloat16
    )
    flat_ids = route_ids.reshape(-1)
    expert_table = (flat_ids[:, None] == jnp.arange(E, dtype=jnp.int32)[None, :]).astype(jnp.int32)
    earlier_count = jnp.cumsum(expert_table, axis=0) - expert_table
    position = jnp.sum(earlier_count * expert_table, axis=1)
    slot_of = flat_ids * CAP + position
    slot_grid = slot_of.reshape(tok_rows, TOPK)
    picker = jnp.any(
        slot_grid[None, :, :] == jnp.arange(E * CAP, dtype=jnp.int32)[:, None, None], axis=2
    ).astype(jnp.bfloat16)
    outgoing = (
        jnp.dot(picker, normed, preferred_element_type=jnp.float32)
        .astype(jnp.bfloat16)
        .reshape(E, CAP, feat_local)
    )
    received = lax.all_gather(
        lax.all_to_all(outgoing, "sp", split_axis=0, concat_axis=0, tiled=True),
        "tp",
        axis=2,
        tiled=True,
    )
    local_experts = gate_experts.shape[0]
    sources = received.shape[0] // local_experts
    count = received.shape[1]
    rows = received.reshape(sources, local_experts, count, received.shape[2])
    gate_pre = jnp.minimum(
        jnp.einsum("sjcd,jdf->sjcf", rows, gate_experts, preferred_element_type=jnp.float32),
        clamp_limit,
    )
    up_pre = jnp.clip(
        jnp.einsum("sjcd,jdf->sjcf", rows, up_experts, preferred_element_type=jnp.float32),
        -clamp_limit,
        clamp_limit,
    )
    hidden = (gate_pre * jax.nn.sigmoid(swish_slope * gate_pre) * (up_pre + 1.0)).astype(
        jnp.bfloat16
    )
    partial_value = jnp.einsum(
        "sjcf,jfd->sjcd", hidden, down_experts, preferred_element_type=jnp.float32
    )
    summed = lax.psum_scatter(
        partial_value.astype(jnp.bfloat16), "tp", scatter_dimension=3, tiled=True
    )
    returned = lax.all_to_all(
        summed.reshape(sources * local_experts, count, summed.shape[3]),
        "sp",
        split_axis=0,
        concat_axis=0,
        tiled=True,
    )
    flat_back = returned.reshape(E * CAP, feat_local)
    picked = flat_back[slot_of].astype(jnp.float32).reshape(tok_rows, TOPK, feat_local)
    routed_sum = jnp.sum(picked * route_weights[:, :, None], axis=1)
    return (middle32 + routed_sum).astype(jnp.bfloat16)


def solution(mesh):
    in_specs = (
        P("sp", "tp"),
        P("sp", "tp"),
        P("sp", "tp"),
        P(None, "tp"),
        P("tp"),
        P("tp", None),
        P(),
        P(None, "tp"),
        P("tp"),
        P("sp", None),
        P("sp", None),
        P("sp", None, "tp"),
        P("sp", None, "tp"),
        P("sp", "tp", None),
    )
    out_specs = P("sp", "tp")
    return jax.shard_map(shards, mesh=mesh, in_specs=in_specs, out_specs=out_specs, check_vma=False)
```

profile of v0, /device:TPU:0, one launch (start us, length us, event | category | flops | bytes accessed | tf_op | source)
XLA Modules:
  0.0 297.5 jit_solution(6796532725709463423)
XLA Ops:
  6.5 1.3 multiply_convert_fusion.2
  7.9 2.4 collective-permute-start
  10.3 1.3 fusion.68
  11.5 1.1 fusion.69
  12.6 2.2 fusion.67
  14.9 10.9 %all-reduce = (f32[192]{0:T(256)S(1)}, f32[192]{0:T(256)S(1)}) all-reduce(f32[192]{0:T(256)S(1)} %get-tuple-element.6, f32[192]{0:T(256)S(1)} %get-tuple-element.5), channel_id=1, replica_groups=mesh['sp'=8,'tp'=4] {'tp'}, use_global_device_ids=true, to_apply=%region_3.0 | all-reduce | flops 384 | bytes 3072 | tf_op jit(solution)/shard_map/psum | solution.py:48
  25.8 2.2 convolution_convert_fusion
  28.5 1.7 reduce-window.6
  31.4 23.3 %reduce-scatter.3.cloned.1.call-done = bf16[48,2048]{1,0:T(8,128)(2,1)} async-done(((bf16[192,2048]{1,0:T(8,128)(2,1)}), bf16[48,2048]{1,0:T(8,128)(2,1)}) %reduce-scatter.3.cloned.1.call-update) | async-done | bytes 196624 | tf_op jit(solution)/shard_map/reduce_scatter | solution.py:54
  56.8 11.2 %all_gather.6 = bf16[192,2048]{1,0:T(8,128)(2,1)S(1)} all-gather(bf16[48,2048]{1,0:T(8,128)(2,1)S(1)} %fusion.24), channel_id=1, replica_groups=mesh['sp'=8,'tp'=4] {'tp'}, dimensions={0}, use_global_device_ids=true | all-gather | bytes 983040 | tf_op jit(solution)/shard_map/all_gather | solution.py:64
  68.0 2.3 multiply_reduce_fusion.1
  70.3 8.9 %psum.23 = f32[192]{0:T(256)S(1)} all-reduce(f32[192]{0:T(256)S(1)} %get-tuple-element.45), channel_id=1, replica_groups=mesh['sp'=8,'tp'=4] {'tp'}, use_global_device_ids=true, to_apply=%region_11.12 | all-reduce | flops 192 | bytes 1536 | tf_op jit(solution)/shard_map/psum | solution.py:71
  79.8 31.1 %all_to_all.10 = bf16[32,32,512]{2,1,0:T(8,128)(2,1)} all-to-all(bf16[32,32,512]{2,1,0:T(8,128)(2,1)S(1)} %bitcast.101), channel_id=1, replica_groups=mesh['sp'=8,'tp'=4] {'sp'}, dimensions={0} | all-to-all | bytes 2097152 | tf_op jit(solution)/shard_map/all_to_all | solution.py:90
  111.1 49.4 %all-gather.2.cloned.1.call-done = bf16[32,32,2048]{2,1,0:T(8,128)(2,1)} async-done(((bf16[32,32,512]{2,1,0:T(8,128)(2,1)}), bf16[32,32,2048]{2,1,0:T(8,128)(2,1)}) %all-gather.2.cloned.1.call-update) | async-done | bytes 4194320 | tf_op jit(solution)/shard_map/all_gather | solution.py:89
  160.5 9.5 %fusion.2 = f32[4,8,32,1024]{3,2,1,0:T(8,128)S(1)} fusion(bf16[4,2048,1024]{2,1,0:T(8,128)(2,1)} %param.26, bf16[8,4,32,2048]{3,2,1,0:T(8,128)(2,1)} %bitcast.134), kind=kOutput, calls=%fused_computation.3 | convolution fusion | flops 4294967296 | bytes 25165824 | tf_op jit(solution)/shard_map/sjcd,jdf->sjcf/dot_general | solution.py:104
  170.1 12.6 %fusion.6 = bf16[8,4,32,1024]{3,2,0,1:T(8,128)(2,1)} fusion(f32[4,8,32,1024]{3,2,1,0:T(8,128)S(1)} %fusion.2, bf16[4,2048,1024]{2,1,0:T(8,128)(2,1)} %param.25, bf16[8,4,32,2048]{3,2,1,0:T(8,128)(2,1)S(1)} %bitcast.135), kind=kOutput, calls=%fused_computation.8 | convolution fusion | flops 4305453056 | bytes 27262976 | tf_op jit(solution)/shard_map/sjcd,jdf->sjcf/dot_general | solution.py:100
  182.7 12.8 %convert_bitcast_fusion = bf16[8,4,32,2048]{3,2,0,1:T(8,128)(2,1)} fusion(bf16[8,4,32,1024]{3,2,0,1:T(8,128)(2,1)} %fusion.6, bf16[4,1024,2048]{2,1,0:T(8,128)(2,1)} %param.27), kind=kOutput, calls=%fused_computation.15 | convolution fusion | flops 4297064448 | bytes 23068672 | tf_op jit(solution)/shard_map/sjcf,jfd->sjcd/dot_general | solution.py:111
  195.6 52.7 %reduce-scatter.5.cloned.1.call-done = bf16[8,4,32,512]{3,2,0,1:T(8,128)(2,1)} async-done(((bf16[8,4,32,2048]{3,2,0,1:T(8,128)(2,1)}), bf16[8,4,32,512]{3,2,0,1:T(8,128)(2,1)}) %reduce-scatter.5.cloned.1.call-update) | async-done | bytes 1048592 | tf_op jit(solution)/shard_map/reduce_scatter | solution.py:114
  248.3 2.3 copy.31
  250.6 4.6 %all-to-all-start.1 = ((bf16[32,32,512]{2,1,0:T(8,128)(2,1)}), bf16[32,32,512]{2,1,0:T(8,128)(2,1)S(1)}, u32[]{:S(2)}, u32[]{:S(2)}) async-start(bf16[32,32,512]{2,1,0:T(8,128)(2,1)} %bitcast.43), calls=%async_computation.3 | async-start | bytes 2097152 | tf_op jit(solution)/shard_map/all_to_all | solution.py:117
  256.2 25.6 %all-to-all-done.1 = bf16[32,32,512]{2,1,0:T(8,128)(2,1)S(1)} async-done(((bf16[32,32,512]{2,1,0:T(8,128)(2,1)}), bf16[32,32,512]{2,1,0:T(8,128)(2,1)S(1)}, u32[]{:S(2)}, u32[]{:S(2)}) %all-to-all-start.1) | async-done | bytes 1048608 | tf_op jit(solution)/shard_map/all_to_all | solution.py:117
  281.8 3.3 %gather_fusion = bf16[768,512]{1,0:T(8,128)(2,1)} fusion(bf16[1024,512]{1,0:T(8,128)(2,1)S(1)} %bitcast.100, s32[1024]{0:T(1024)S(1)} %pad_clamp_fusion), kind=kCustom, calls=%fused_computation | custom fusion | bytes 1575936 | tf_op jit(solution)/shard_map/gather | solution.py:125
  285.1 2.6 reshape.93
  287.7 2.5 multiply_reduce_fusion
  (46 shorter events, 6.2 us)
Async XLA Ops:
  6.5 19.2 %copy-start = (bf16[512,2048]{1,0:T(8,128)(2,1)S(1)}, bf16[512,2048]{1,0:T(8,128)(2,1)}, u32[]{:S(2)}) copy-start(bf16[512,2048]{1,0:T(8,128)(2,1)} %param.19) | copy-start | bytes 6291460
  6.5 21.5 %copy-start.4 = (s32[192,4]{0,1:T(4,128)S(1)}, s32[192,4]{0,1:T(4,128)}, u32[]{:S(2)}) copy-start(s32[192,4]{0,1:T(4,128)} %param.23) | copy-start | bytes 9220
  6.5 49.3 %copy-start.3 = (f32[2048]{0:T(1024)S(1)}, f32[2048]{0:T(1024)}, u32[]{:S(2)}) copy-start(f32[2048]{0:T(1024)} %param.20) | copy-start | bytes 24580
  6.5 48.2 %reduce-scatter.3.cloned.1.call-start = ((), (), s32[]{:S(2)}) async-start(), calls=%async_computation.4 | async-start | bytes 983040 | tf_op jit(solution)/shard_map/reduce_scatter | solution.py:54
  7.9 4.8 %collective-permute-start = (bf16[30,512]{1,0:T(8,128)(2,1)S(1)}, bf16[30,512]{1,0:T(8,128)(2,1)S(1)}, u32[]{:S(2)}, u32[]{:S(2)}) collective-permute-start(bf16[30,512]{1,0:T(8,128)(2,1)S(1)} %slice.258), channel_id=1, source_target_pairs={{0,4},{4,8},{8,12},{12,16},{16,20},{20,24},{24,28},{1,5},{5,9},{9,... | collective-permute-start | bytes 92168 | tf_op jit(solution)/shard_map/ppermute | solution.py:17
  14.9 53.2 %copy-start.2 = (bf16[192,512]{1,0:T(8,128)(2,1)S(1)}, bf16[192,512]{1,0:T(8,128)(2,1)}, u32[]{:S(2)}) copy-start(bf16[192,512]{1,0:T(8,128)(2,1)} %param.14) | copy-start | bytes 589828
  28.0 51.2 %copy-start.6 = (f32[512]{0:T(512)S(1)}, f32[512]{0:T(512)}, u32[]{:S(2)}) copy-start(f32[512]{0:T(512)} %param.22) | copy-start | bytes 6148
  28.0 132.5 %all-gather.2.cloned.1.call-start = ((), (), s32[]{:S(2)}) async-start(), calls=%async_computation.5 | async-start | bytes 5242880 | tf_op jit(solution)/shard_map/all_gather | solution.py:89
  110.9 137.4 %reduce-scatter.5.cloned.1.call-start = ((), (), s32[]{:S(2)}) async-start(), calls=%async_computation.6 | async-start | bytes 5242880 | tf_op jit(solution)/shard_map/reduce_scatter | solution.py:114
  160.5 9.5 %copy-start.7 = (bf16[32,32,2048]{2,1,0:T(8,128)(2,1)S(1)}, bf16[32,32,2048]{2,1,0:T(8,128)(2,1)}, u32[]{:S(2)}) copy-start(bf16[32,32,2048]{2,1,0:T(8,128)(2,1)} %all-gather.2.cloned.1.call-done) | copy-start | bytes 12582916
  195.6 59.8 %copy-start.5 = (f32[192,4]{0,1:T(4,128)S(1)}, f32[192,4]{0,1:T(4,128)}, u32[]{:S(2)}) copy-start(f32[192,4]{0,1:T(4,128)} %param.24) | copy-start | bytes 9220
  250.6 31.2 %all-to-all-start.1 = ((bf16[32,32,512]{2,1,0:T(8,128)(2,1)}), bf16[32,32,512]{2,1,0:T(8,128)(2,1)S(1)}, u32[]{:S(2)}, u32[]{:S(2)}) async-start(bf16[32,32,512]{2,1,0:T(8,128)(2,1)} %bitcast.43), calls=%async_computation.3 | async-start | bytes 2097152 | tf_op jit(solution)/shard_map/all_to_all | solution.py:117
  281.8 9.1 %copy-start.1 = (bf16[512,2048]{1,0:T(8,128)(2,1)S(1)}, bf16[512,2048]{1,0:T(8,128)(2,1)}, u32[]{:S(2)}) copy-start(bf16[512,2048]{1,0:T(8,128)(2,1)} %param.19) | copy-start | bytes 6291460
Sparse Core Ops, SparseCore 0:
  28.2 26.5 reduce-scatter.2
  111.0 49.4 all-gather.1
  195.7 52.5 reduce-scatter.4
where the time goes:
time: 298 us; the launch traced here: 297 us
  waiting for transfers between devices  151 us (51%)
  blocking collectives  62 us (21%)
  matrix products  40.1 us (13%)
  between operations  13.3 us (4%)
  local copies, waits for them, and re-layouts  12.3 us (4%)
  other arithmetic  11.3 us (4%)
  starting transfers between devices  7.27 us (2%)
    reduce_scatter x1, waiting for transfers between devices, shards(): lax.psum_scatter(partial_value.astype(jnp.bfloat16), 'tp', scatter_dimens...  52.7 us
    all_gather x1, waiting for transfers between devices, shards(): lax.all_gather(lax.all_to_all(outgoing, 'sp', split_axis=0, concat_axis=0...  49.4 us
    all_to_all x1, blocking collectives, shards(): lax.all_to_all(outgoing, 'sp', split_axis=0, concat_axis=0, tiled=True)  31.1 us
    all_to_all x1, waiting for transfers between devices, shards(): lax.all_to_all(summed.reshape(sources * local_experts, count, summed.shap...  25.6 us
    reduce_scatter x1, waiting for transfers between devices, shards(): lax.psum_scatter(jnp.dot(act, point_weight, preferred_element_type=jnp.fl...  23.3 us
    dot_general x1, matrix products, shards(): jnp.einsum('sjcf,jfd->sjcd', hidden, down_experts, preferred_element_type...  12.8 us
    dot_general x1, matrix products, shards(): jnp.einsum('sjcd,jdf->sjcf', rows, gate_experts, preferred_element_type=j...  12.6 us
    all_gather x1, blocking collectives, shards(): lax.all_gather(mixed, 'tp', axis=0, tiled=True)  11.2 us
  transfers between devices with their start and end apart: 5, of which 4 were waited for; matrix products, arithmetic and copies ran while one was open for 2% of the time, Pallas kernels for 0%

commit v1 on v0

--- a/solution.py
+++ b/solution.py
@@ -86,11 +86,11 @@
         .astype(jnp.bfloat16)
         .reshape(E, CAP, feat_local)
     )
-    received = lax.all_gather(
-        lax.all_to_all(outgoing, "sp", split_axis=0, concat_axis=0, tiled=True),
-        "tp",
+    received = jnp.concatenate(
+        lax.all_gather(
+            lax.all_to_all(outgoing, "sp", split_axis=0, concat_axis=0, tiled=True), "tp"
+        ),
         axis=2,
-        tiled=True,
     )
     local_experts = gate_experts.shape[0]
     sources = received.shape[0] // local_experts

time: 298 us -> 312 us (1.047)
  local copies, waits for them, and re-layouts: 12.3 us -> 28.2 us
    reshape x0 -> x1, local copies, waits for them, and re-layouts: none -> 8.12 us  [shards(): jnp.concatenate(lax.all_gather(lax.all_to_all(outgoing, 'sp', split_axis=...]
    another operation x0 -> x1, local copies, waits for them, and re-layouts: none -> 7.75 us  [shards(): rows = received.reshape(sources, local_experts, count, received.shape[2])]
where the time goes in v1:
time: 312 us; the launch traced here: 311 us
  waiting for transfers between devices  152 us (49%)
  blocking collectives  62 us (20%)
  matrix products  37.8 us (12%)
  local copies, waits for them, and re-layouts  28.2 us (9%)
  between operations  13.3 us (4%)
  other arithmetic  11.3 us (4%)
  starting transfers between devices  7.09 us (2%)
    reduce_scatter x1, waiting for transfers between devices, shards(): lax.psum_scatter(partial_value.astype(jnp.bfloat16), 'tp', scatter_dimens...  52.8 us
    all_gather x1, waiting for transfers between devices, shards(): lax.all_gather(lax.all_to_all(outgoing, 'sp', split_axis=0, concat_axis=0...  49.7 us
    all_to_all x1, blocking collectives, shards(): lax.all_to_all(outgoing, 'sp', split_axis=0, concat_axis=0, tiled=True)  31.1 us
    all_to_all x1, waiting for transfers between devices, shards(): lax.all_to_all(summed.reshape(sources * local_experts, count, summed.shap...  25.6 us
    reduce_scatter x1, waiting for transfers between devices, shards(): lax.psum_scatter(jnp.dot(act, point_weight, preferred_element_type=jnp.fl...  23.3 us
    dot_general x1, matrix products, shards(): jnp.einsum('sjcf,jfd->sjcd', hidden, down_experts, preferred_element_type...  11.9 us
    dot_general x1, matrix products, shards(): jnp.einsum('sjcd,jdf->sjcf', rows, gate_experts, preferred_element_type=j...  11.3 us
    all_gather x1, blocking collectives, shards(): lax.all_gather(mixed, 'tp', axis=0, tiled=True)  11.2 us
  transfers between devices with their start and end apart: 5, of which 4 were waited for; matrix products, arithmetic and copies ran while one was open for 2% of the time, Pallas kernels for 0%

profile of v1, /device:TPU:0, one launch (start us, length us, event | category | flops | bytes accessed | tf_op | source)
XLA Modules:
  0.0 311.2 jit_solution(3439611317738213485)
XLA Ops:
  6.5 1.3 multiply_convert_fusion.2
  7.9 2.4 collective-permute-start
  12.6 2.2 fusion.67
  14.9 10.9 %all-reduce = (f32[192]{0:T(256)S(1)}, f32[192]{0:T(256)S(1)}) all-reduce(f32[192]{0:T(256)S(1)} %get-tuple-element.6, f32[192]{0:T(256)S(1)} %get-tuple-element.5), channel_id=1, replica_groups=mesh['sp'=8,'tp'=4] {'tp'}, use_global_device_ids=true, to_apply=%region_3.0 | all-reduce | flops 384 | bytes 3072 | tf_op jit(solution)/shard_map/psum | solution.py:48
  25.8 2.2 convolution_convert_fusion
  28.5 1.7 reduce-window.6
  31.4 23.3 %reduce-scatter.3.cloned.1.call-done = bf16[48,2048]{1,0:T(8,128)(2,1)} async-done(((bf16[192,2048]{1,0:T(8,128)(2,1)}), bf16[48,2048]{1,0:T(8,128)(2,1)}) %reduce-scatter.3.cloned.1.call-update) | async-done | bytes 196624 | tf_op jit(solution)/shard_map/reduce_scatter | solution.py:54
  56.8 11.2 %all_gather.9 = bf16[192,2048]{1,0:T(8,128)(2,1)S(1)} all-gather(bf16[48,2048]{1,0:T(8,128)(2,1)S(1)} %fusion.24), channel_id=1, replica_groups=mesh['sp'=8,'tp'=4] {'tp'}, dimensions={0}, use_global_device_ids=true | all-gather | bytes 983040 | tf_op jit(solution)/shard_map/all_gather | solution.py:64
  68.0 2.3 multiply_reduce_fusion.1
  70.3 8.9 %psum.23 = f32[192]{0:T(256)S(1)} all-reduce(f32[192]{0:T(256)S(1)} %get-tuple-element.45), channel_id=1, replica_groups=mesh['sp'=8,'tp'=4] {'tp'}, use_global_device_ids=true, to_apply=%region_11.12 | all-reduce | flops 192 | bytes 1536 | tf_op jit(solution)/shard_map/psum | solution.py:71
  79.8 31.1 %all_to_all.10 = bf16[32,32,512]{2,1,0:T(8,128)(2,1)} all-to-all(bf16[32,32,512]{2,1,0:T(8,128)(2,1)S(1)} %bitcast.104), channel_id=1, replica_groups=mesh['sp'=8,'tp'=4] {'sp'}, dimensions={0} | all-to-all | bytes 2097152 | tf_op jit(solution)/shard_map/all_to_all | solution.py:91
  110.9 49.7 %all-gather.3.cloned.1.call-done = bf16[128,32,512]{2,1,0:T(8,128)(2,1)} async-done(((bf16[32,32,512]{2,1,0:T(8,128)(2,1)}), bf16[128,32,512]{2,1,0:T(8,128)(2,1)}) %all-gather.3.cloned.1.call-update) | async-done | bytes 4194320 | tf_op jit(solution)/shard_map/all_gather | solution.py:90
  160.7 8.1 %copy.47 = bf16[32,32,4,512]{3,2,1,0:T(4,128)(2,1)} copy(bf16[32,32,4,512]{3,1,0,2:T(8,128)(2,1)} %bitcast.103) | data formatting | bytes 8388608 | tf_op jit(solution)/shard_map/reshape | solution.py:89
  168.8 7.7 %reshape_reshape.3 = bf16[8,4,32,2048]{3,2,1,0:T(8,128)(2,1)} reshape(bf16[32,32,4,512]{3,2,1,0:T(4,128)(2,1)} %copy.47) | data formatting | bytes 8388608 | tf_op jit(solution)/shard_map/reshape;reshape | solution.py:98
  176.5 9.5 %fusion.2 = f32[4,8,32,1024]{3,2,1,0:T(8,128)S(1)} fusion(bf16[4,2048,1024]{2,1,0:T(8,128)(2,1)} %param.26, bf16[8,4,32,2048]{3,2,1,0:T(8,128)(2,1)} %reshape_reshape.3), kind=kOutput, calls=%fused_computation.3 | convolution fusion | flops 4294967296 | bytes 25165824 | tf_op jit(solution)/shard_map/sjcd,jdf->sjcf/dot_general | solution.py:104
  186.1 11.3 %fusion.6 = bf16[8,4,32,1024]{3,2,0,1:T(8,128)(2,1)S(1)} fusion(f32[4,8,32,1024]{3,2,1,0:T(8,128)S(1)} %fusion.2, bf16[4,2048,1024]{2,1,0:T(8,128)(2,1)} %param.25, bf16[8,4,32,2048]{3,2,1,0:T(8,128)(2,1)S(1)} %copy-done.2), kind=kOutput, calls=%fused_computation.8 | convolution fusion | flops 4305453056 | bytes 27262976 | tf_op jit(solution)/shard_map/sjcd,jdf->sjcf/dot_general | solution.py:100
  197.4 11.9 %convert_bitcast_fusion = bf16[8,4,32,2048]{3,2,0,1:T(8,128)(2,1)} fusion(bf16[8,4,32,1024]{3,2,0,1:T(8,128)(2,1)S(1)} %fusion.6, bf16[4,1024,2048]{2,1,0:T(8,128)(2,1)} %param.27), kind=kOutput, calls=%fused_computation.15 | convolution fusion | flops 4297064448 | bytes 23068672 | tf_op jit(solution)/shard_map/sjcf,jfd->sjcd/dot_general | solution.py:111
  209.3 52.8 %reduce-scatter.5.cloned.1.call-done = bf16[8,4,32,512]{3,2,0,1:T(8,128)(2,1)} async-done(((bf16[8,4,32,2048]{3,2,0,1:T(8,128)(2,1)}), bf16[8,4,32,512]{3,2,0,1:T(8,128)(2,1)}) %reduce-scatter.5.cloned.1.call-update) | async-done | bytes 1048592 | tf_op jit(solution)/shard_map/reduce_scatter | solution.py:114
  262.1 2.3 copy.50
  264.4 4.6 %all-to-all-start.1 = ((bf16[32,32,512]{2,1,0:T(8,128)(2,1)}), bf16[32,32,512]{2,1,0:T(8,128)(2,1)S(1)}, u32[]{:S(2)}, u32[]{:S(2)}) async-start(bf16[32,32,512]{2,1,0:T(8,128)(2,1)} %bitcast.44), calls=%async_computation.3 | async-start | bytes 2097152 | tf_op jit(solution)/shard_map/all_to_all | solution.py:117
  269.9 25.6 %all-to-all-done.1 = bf16[32,32,512]{2,1,0:T(8,128)(2,1)S(1)} async-done(((bf16[32,32,512]{2,1,0:T(8,128)(2,1)}), bf16[32,32,512]{2,1,0:T(8,128)(2,1)S(1)}, u32[]{:S(2)}, u32[]{:S(2)}) %all-to-all-start.1) | async-done | bytes 1048608 | tf_op jit(solution)/shard_map/all_to_all | solution.py:117
  295.6 3.3 %gather_fusion = bf16[768,512]{1,0:T(8,128)(2,1)} fusion(bf16[1024,512]{1,0:T(8,128)(2,1)S(1)} %bitcast.102, s32[1024]{0:T(1024)S(1)} %pad_clamp_fusion), kind=kCustom, calls=%fused_computation | custom fusion | bytes 1575936 | tf_op jit(solution)/shard_map/gather | solution.py:125
  298.9 2.6 reshape.93
  301.5 2.5 multiply_reduce_fusion
  (48 shorter events, 8.4 us)
Async XLA Ops:
  6.5 19.2 %copy-start = (bf16[512,2048]{1,0:T(8,128)(2,1)S(1)}, bf16[512,2048]{1,0:T(8,128)(2,1)}, u32[]{:S(2)}) copy-start(bf16[512,2048]{1,0:T(8,128)(2,1)} %param.19) | copy-start | bytes 6291460
  6.5 21.5 %copy-start.5 = (s32[192,4]{0,1:T(4,128)S(1)}, s32[192,4]{0,1:T(4,128)}, u32[]{:S(2)}) copy-start(s32[192,4]{0,1:T(4,128)} %param.23) | copy-start | bytes 9220
  6.5 49.3 %copy-start.4 = (f32[2048]{0:T(1024)S(1)}, f32[2048]{0:T(1024)}, u32[]{:S(2)}) copy-start(f32[2048]{0:T(1024)} %param.20) | copy-start | bytes 24580
  6.5 48.2 %reduce-scatter.3.cloned.1.call-start = ((), (), s32[]{:S(2)}) async-start(), calls=%async_computation.4 | async-start | bytes 983040 | tf_op jit(solution)/shard_map/reduce_scatter | solution.py:54
  7.9 4.8 %collective-permute-start = (bf16[30,512]{1,0:T(8,128)(2,1)S(1)}, bf16[30,512]{1,0:T(8,128)(2,1)S(1)}, u32[]{:S(2)}, u32[]{:S(2)}) collective-permute-start(bf16[30,512]{1,0:T(8,128)(2,1)S(1)} %slice.258), channel_id=1, source_target_pairs={{0,4},{4,8},{8,12},{12,16},{16,20},{20,24},{24,28},{1,5},{5,9},{9,... | collective-permute-start | bytes 92168 | tf_op jit(solution)/shard_map/ppermute | solution.py:17
  14.9 53.2 %copy-start.3 = (bf16[192,512]{1,0:T(8,128)(2,1)S(1)}, bf16[192,512]{1,0:T(8,128)(2,1)}, u32[]{:S(2)}) copy-start(bf16[192,512]{1,0:T(8,128)(2,1)} %param.14) | copy-start | bytes 589828
  28.0 51.2 %copy-start.7 = (f32[512]{0:T(512)S(1)}, f32[512]{0:T(512)}, u32[]{:S(2)}) copy-start(f32[512]{0:T(512)} %param.22) | copy-start | bytes 6148
  28.0 132.6 %all-gather.3.cloned.1.call-start = ((), (), s32[]{:S(2)}) async-start(), calls=%async_computation.6 | async-start | bytes 5242880 | tf_op jit(solution)/shard_map/all_gather | solution.py:90
  110.9 151.2 %reduce-scatter.5.cloned.1.call-start = ((), (), s32[]{:S(2)}) async-start(), calls=%async_computation.5 | async-start | bytes 5242880 | tf_op jit(solution)/shard_map/reduce_scatter | solution.py:114
  176.5 9.5 %copy-start.2 = (bf16[8,4,32,2048]{3,2,1,0:T(8,128)(2,1)S(1)}, bf16[8,4,32,2048]{3,2,1,0:T(8,128)(2,1)}, u32[]{:S(2)}) copy-start(bf16[8,4,32,2048]{3,2,1,0:T(8,128)(2,1)} %reshape_reshape.3) | copy-start | bytes 12582916
  209.3 59.8 %copy-start.6 = (f32[192,4]{0,1:T(4,128)S(1)}, f32[192,4]{0,1:T(4,128)}, u32[]{:S(2)}) copy-start(f32[192,4]{0,1:T(4,128)} %param.24) | copy-start | bytes 9220
  264.4 31.2 %all-to-all-start.1 = ((bf16[32,32,512]{2,1,0:T(8,128)(2,1)}), bf16[32,32,512]{2,1,0:T(8,128)(2,1)S(1)}, u32[]{:S(2)}, u32[]{:S(2)}) async-start(bf16[32,32,512]{2,1,0:T(8,128)(2,1)} %bitcast.44), calls=%async_computation.3 | async-start | bytes 2097152 | tf_op jit(solution)/shard_map/all_to_all | solution.py:117
  295.6 9.1 %copy-start.1 = (bf16[512,2048]{1,0:T(8,128)(2,1)S(1)}, bf16[512,2048]{1,0:T(8,128)(2,1)}, u32[]{:S(2)}) copy-start(bf16[512,2048]{1,0:T(8,128)(2,1)} %param.19) | copy-start | bytes 6291460
Sparse Core Ops, SparseCore 0:
  28.2 26.5 reduce-scatter.2
  111.0 49.6 all-gather.2
  209.4 52.5 reduce-scatter.4
